TPU v7x, 256 devices: a 4x2x16 block of a 4x16x16 slice. The times are simulated.
256 devices in a mesh: grp: 2 (over y), sp: 32 (over z, core), tp: 4 (over x).
Axes of the slice: x: 4, y: 2, z: 16, core: 2. Of those that a mesh axis runs over, the one named last changes fastest.
The devices are a block of a 4x16x16 slice.
Arguments:
- residual_in: bfloat16 [16384, 2048], P(('grp', 'sp', 'tp')), parts along dimension 0, may hold values from -1.1953125 to 1.1953125
- query_small: bfloat16 [16384, 1024], P(('grp', 'sp'), 'tp'), parts along dimension 0, may hold values from -6 to 6
- query_large: bfloat16 [16384, 1024], P(('grp', 'sp'), 'tp'), parts along dimension 0, may hold values from -6 to 6
- key_small: bfloat16 [64, 16384], P(None, ('grp', 'sp')), parts along dimension 1, may hold values from -6 to 6
- key_large: bfloat16 [128, 16384], P(None, ('grp', 'sp')), parts along dimension 1, may hold values from -6 to 6
- value_small: bfloat16 [64, 16384], P(None, ('grp', 'sp')), parts along dimension 1, may hold values from -6 to 6
- value_large: bfloat16 [128, 16384], P(None, ('grp', 'sp')), parts along dimension 1, may hold values from -6 to 6
- forget_small: float32 [16, 16384], P('tp', ('grp', 'sp')), parts along dimension 1, may hold values from -1172 to 0, as said below
- forget_large: float32 [8, 16384], P('tp', ('grp', 'sp')), parts along dimension 1, may hold values from -1172 to 0, as said below
- project_small: bfloat16 [1024, 2048], P('tp'), may hold values from -0.125 to 0.125
- project_large: bfloat16 [1024, 2048], P('tp'), may hold values from -0.125 to 0.125
- norm_gain: bfloat16 [2048], replicated, may hold values from 0.099609375 to 1.8984375
- expert_gate: bfloat16 [128, 2048, 512], P(('sp', 'tp')), may hold values from -0.125 to 0.125
- expert_up: bfloat16 [128, 2048, 512], P(('sp', 'tp')), may hold values from -0.125 to 0.125
- expert_down: bfloat16 [128, 512, 2048], P(('sp', 'tp')), may hold values from -0.25 to 0.25
- routing: int32 [16384, 2], P(('grp', 'sp', 'tp')), parts along dimension 0, may hold values from 0 to 127, all different within a row; in each aligned block of 64 rows (0 to 63, 64 to 127, ...) at most 2 rows name the same one
- route_weight: float32 [16384, 2], P(('grp', 'sp', 'tp')), parts along dimension 0, may hold values from 0.2 to 1
Outputs:
- layer_out: bfloat16 [16384, 2048], P(('grp', 'sp', 'tp')), parts along dimension 0
There are 2 independent parts, one for each index of `grp`. A program takes and returns all parts, laid end to end along the dimension named above; an argument that names none is the same for every part. Nothing has to cross between parts.
Inputs may be any that keep to these rules, and one draw needn't show every extreme that they name: `forget_small`: each row never rises from one position to the next. `forget_large`: each row never rises from one position to the next. `routing`: each row names 2 different experts; in the rows of one device no expert is named by more than 2 rows, and in some devices' rows some expert is named by exactly 2.
All inputs are finite; a program needn't handle non-finite values.
Results may differ from a plain program's by a relative error of at most 0.018.
Values may be sent and summed in bfloat16 or wider, within the bound.
No kernel may reach another device: no remote copies, remote signals or barrier semaphores. Data moves between devices by JAX's collectives and lax.ppermute only.
A program may use at most 64 MiB of HBM per device.

v0:
```python
import math

import jax
import jax.numpy as jnp
from jax import lax
from jax.experimental import pallas as pl
from jax.experimental.pallas import tpu as pltpu
from jax.sharding import PartitionSpec as P


BF = jnp.bfloat16
F32 = jnp.float32
LOG2E = math.log2(math.e)
GATE_ROWS = 16
PIECES = 3
LOW = -1e30


def params(mib=16):
    return pltpu.CompilerParams(vmem_limit_bytes=mib << 20)


def packed(keys_values, gates, size_s, size_l, heads_s):
    at_l = size_s + GATE_ROWS
    at_v = at_l + size_l + GATE_ROWS

    def body(kv, gate, out):
        def pieces(left, size):
            left = left * -(size**0.5)
            rows = []
            for _ in range(PIECES):
                piece = left.astype(BF).astype(F32)
                rows.append(piece)
                left = left - piece
            used = PIECES * left.shape[0]
            rows.append(jnp.zeros((GATE_ROWS - used, left.shape[1]), F32))
            return jnp.concatenate(rows, axis=0).astype(BF)

        out[:size_s] = kv[:size_s]
        out[size_s:at_l] = pieces(gate[:heads_s], size_s)
        out[at_l : at_l + size_l] = kv[size_s : size_s + size_l]
        out[at_l + size_l : at_v] = pieces(gate[heads_s:], size_l)
        out[at_v:] = kv[size_s + size_l :]

    return pl.pallas_call(
        body,
        out_shape=jax.ShapeDtypeStruct((at_v + size_s + size_l, keys_values.shape[1]), BF),
        compiler_params=params(),
        name="packed",
    )(keys_values, gates)


def update(units, keys, values, size, keep=None):
    factor = LOG2E * size**-0.5
    rows = size + GATE_ROWS
    tops = [state[h, rows : rows + 1] for _, state, h in units]

    def scores(i):
        q, _, h = units[i]
        s = jnp.dot(keys[...], q[h], preferred_element_type=F32)
        return s if keep is None else jnp.where(keep, s, LOW)

    s = scores(0)
    for i, (_, state, h) in enumerate(units):
        following = scores(i + 1) if i + 1 < len(units) else None
        new = jnp.maximum(tops[i], jnp.max(s, axis=0, keepdims=True))
        p = jnp.exp2((s - new) * factor).astype(BF)
        alpha = jnp.exp2((tops[i] - new) * factor)
        mixed = jnp.dot(values[...], p, preferred_element_type=F32)
        state[h, :rows] = state[h, :rows] * alpha + mixed
        state[h, rows:] = jnp.broadcast_to(new, (state.shape[1] - rows, new.shape[1]))
        s = following


def lay_out(blocks, ks, vs, kl, vl):
    size_s, size_l = ks.shape[1] - GATE_ROWS, kl.shape[1] - GATE_ROWS
    a = size_s + GATE_ROWS
    b = a + size_l + GATE_ROWS
    for i, block in enumerate(blocks):
        count = block.shape[1]
        at = pl.ds(i * count, count)
        ks[at] = block[0:a].T
        kl[at] = block[a:b].T
        vs[:size_s, at] = block[b : b + size_s]
        vl[:size_l, at] = block[b + size_s :]
    vs[size_s:] = jnp.ones((GATE_ROWS, vs.shape[1]), BF)
    vl[size_l:] = jnp.ones((GATE_ROWS, vl.shape[1]), BF)


def add_keys(sets, ks, vs, kl, vl, keep=None, together=1):
    def heads(which, keys, values):
        size = keys.shape[1] - GATE_ROWS
        count = sets[0][which].shape[0]
        group = math.gcd(together, count)

        def some(i, carry):
            units = [(one[which], one[which + 2], i * group + k) for k in range(group) for one in sets]
            update(units, keys, values, size, keep)
            return carry

        if count == group:
            some(0, 0)
        else:
            lax.fori_loop(0, count // group, some, 0)

    heads(0, ks, vs)
    heads(1, kl, vl)


def key_scratch(size_s, size_l, count):
    return [
        pltpu.VMEM((count, size_s + GATE_ROWS), BF),
        pltpu.VMEM((size_s + GATE_ROWS, count), BF),
        pltpu.VMEM((count, size_l + GATE_ROWS), BF),
        pltpu.VMEM((size_l + GATE_ROWS, count), BF),
    ]


def first_body(info, own_s, own_l, peer_s, peer_l, block, qs_o, ql_o, qs_p, ql_p, ss_o, sl_o, ss_p, sl_p, *laid):
    tokens = own_s.shape[0]

    def spread(queries, out):
        heads, width, _ = out.shape
        size = width - GATE_ROWS
        turned = queries[...].T
        row = lax.broadcasted_iota(jnp.int32, (GATE_ROWS, tokens), 0)
        for h in range(heads):
            chosen = (row % heads == h) & (row < PIECES * heads)
            out[h, :size] = turned[h * size : (h + 1) * size]
            out[h, size:] = jnp.where(chosen, 1.0, 0.0).astype(BF)

    lay_out([block], *laid)
    spread(own_s, qs_o)
    spread(own_l, ql_o)
    spread(peer_s, qs_p)
    spread(peer_l, ql_p)
    for state in (ss_o, sl_o, ss_p, sl_p):
        heads, rows, _ = state.shape
        state[:, : rows - 8] = jnp.zeros((heads, rows - 8, tokens), F32)
        state[:, rows - 8 :] = jnp.full((heads, 8, tokens), LOW, F32)
    shape = (block.shape[1], tokens)
    keep = lax.broadcasted_iota(jnp.int32, shape, 1) >= lax.broadcasted_iota(jnp.int32, shape, 0)
    add_keys([(qs_o, ql_o, ss_o, sl_o)], *laid, keep=keep)

    @pl.when(info[0] == 1)
    def _():
        add_keys([(qs_p, ql_p, ss_p, sl_p)], *laid)


def first(info, own_s, own_l, peer_s, peer_l, block, heads_s, heads_l):
    tokens = own_s.shape[0]
    size_s, size_l = own_s.shape[1] // heads_s, own_l.shape[1] // heads_l
    vm = pl.BlockSpec(memory_space=pltpu.VMEM)
    queries = [
        jax.ShapeDtypeStruct((heads_s, size_s + GATE_ROWS, tokens), BF),
        jax.ShapeDtypeStruct((heads_l, size_l + GATE_ROWS, tokens), BF),
    ]
    states = [
        jax.ShapeDtypeStruct((heads_s, size_s + GATE_ROWS + 8, tokens), F32),
        jax.ShapeDtypeStruct((heads_l, size_l + GATE_ROWS + 8, tokens), F32),
    ]
    return pl.pallas_call(
        first_body,
        in_specs=[pl.BlockSpec(memory_space=pltpu.SMEM)] + [vm] * 5,
        out_specs=[vm] * 8,
        out_shape=queries * 2 + states * 2,
        scratch_shapes=key_scratch(size_s, size_l, block.shape[1]),
        compiler_params=params(),
        name="first",
    )(info, own_s, own_l, peer_s, peer_l, block)


def advance(info, step, queries, blocks, states):
    def body(flags, qs_o, ql_o, qs_p, ql_p, *refs):
        arrived, (ss_o, sl_o, ss_p, sl_p), laid = refs[: len(blocks)], refs[-8:-4], refs[-4:]

        @pl.when(flags[step] == 1)
        def _():
            lay_out(arrived, *laid)
            add_keys([(qs_o, ql_o, ss_o, sl_o), (qs_p, ql_p, ss_p, sl_p)], *laid)

    vm = pl.BlockSpec(memory_space=pltpu.VMEM)
    at = 1 + len(queries) + len(blocks)
    size_s, size_l = queries[0].shape[1] - GATE_ROWS, queries[1].shape[1] - GATE_ROWS
    return pl.pallas_call(
        body,
        in_specs=[pl.BlockSpec(memory_space=pltpu.SMEM)] + [vm] * (at - 1 + len(states)),
        out_specs=[vm] * len(states),
        out_shape=[jax.ShapeDtypeStruct(s.shape, s.dtype) for s in states],
        input_output_aliases={at + i: i for i in range(len(states))},
        scratch_shapes=key_scratch(size_s, size_l, sum(b.shape[1] for b in blocks)),
        compiler_params=params(),
    )(info, *queries, *blocks, *states)


def finish_body(own_s, own_l, got_s, got_l, project_s, project_l, out):
    def attended(own, got):
        heads, rows, _ = own.shape
        size = rows - 8 - GATE_ROWS
        factor = LOG2E * size**-0.5
        done = []
        for h in range(heads):
            a, b = own[h, rows - 8 : rows - 7], got[h, rows - 8 : rows - 7]
            top = jnp.maximum(a, b)
            wa, wb = jnp.exp2((a - top) * factor), jnp.exp2((b - top) * factor)
            total = own[h, size : size + 1] * wa + got[h, size : size + 1] * wb
            sums = own[h, :size] * wa + got[h, :size] * wb
            done.append((sums / total).astype(BF))
        return jnp.concatenate(done, axis=0).T

    total = jnp.dot(attended(own_s, got_s), project_s[...], preferred_element_type=F32)
    total = total + jnp.dot(attended(own_l, got_l), project_l[...], preferred_element_type=F32)
    out[...] = total.astype(BF)


def finish(own_s, own_l, got_s, got_l, project_s, project_l):
    return pl.pallas_call(
        finish_body,
        out_shape=jax.ShapeDtypeStruct((own_s.shape[2], project_s.shape[1]), BF),
        compiler_params=params(),
        name="finish",
    )(own_s, own_l, got_s, got_l, project_s, project_l)


def attend_and_project(qs, ql, key_small, key_large, value_small, value_large, gs, gl, ps, pb):
    devices = lax.axis_size("sp")
    chips = devices // 2
    place = lax.axis_index("sp").astype(jnp.int32)
    chip, core = place // 2, place % 2
    swap = [(i, i ^ 1) for i in range(devices)]
    ring = [(i, (i + 2 - 4 * (i % 2)) % devices) for i in range(devices)]
    steps = chips // 2
    k = jnp.arange(1, steps + 1, dtype=jnp.int32)
    usable = jnp.where(core == 0, chip >= k, chip + k >= chips).astype(jnp.int32)
    info = jnp.concatenate([(1 - core).reshape(1), usable])

    peer_s = lax.ppermute(qs, "sp", swap)
    peer_l = lax.ppermute(ql, "sp", swap)
    kv = jnp.concatenate([key_small, key_large, value_small, value_large], axis=0)
    gates = jnp.concatenate([gs, gl], axis=0)
    block = packed(kv, gates, key_small.shape[0], key_large.shape[0], gs.shape[0])
    b = lax.ppermute(block, "sp", swap)
    a = block
    made = first(info, qs, ql, peer_s, peer_l, block, gs.shape[0], gl.shape[0])
    queries, states = made[:4], made[4:]
    for step in range(1, steps + 1):
        a = lax.ppermute(a, "sp", ring)
        blocks = [a]
        if step < steps or chips % 2:
            b = lax.ppermute(b, "sp", ring)
            blocks.append(b)
        states = advance(info, step, queries, blocks, states)
    got_s = lax.ppermute(states[2], "sp", swap)
    got_l = lax.ppermute(states[3], "sp", swap)
    return finish(states[0], states[1], got_s, got_l, ps, pb)


def mix_body(parts, residual_in, gain, slots, resid_out, outgoing):
    projected = parts[0].astype(F32)
    for i in range(1, parts.shape[0]):
        projected = projected + parts[i].astype(F32)
    resid = residual_in[...].astype(F32) + projected
    resid_out[...] = resid
    scale = lax.rsqrt(jnp.mean(resid * resid, axis=1, keepdims=True) + 1e-06)
    normed = (resid * scale * gain[...].astype(F32)).astype(BF)
    outgoing[...] = jnp.dot(slots[...], normed, preferred_element_type=F32).astype(BF)


def mix(parts, residual_in, gain, slots):
    rows, width = residual_in.shape
    return pl.pallas_call(
        mix_body,
        out_shape=(
            jax.ShapeDtypeStruct((rows, width), F32),
            jax.ShapeDtypeStruct((slots.shape[0], width), BF),
        ),
        compiler_params=params(),
        name="mix",
    )(parts, residual_in, gain, slots)


def expert_body(rows, gate, up, down, out, total):
    step = pl.program_id(0)
    g = jnp.dot(rows[...], gate[0], preferred_element_type=F32)
    u = jnp.dot(rows[...], up[0], preferred_element_type=F32)
    hidden = (g / (1.0 + jnp.exp(-g)) * u).astype(BF)
    width = out.shape[1]
    span = math.gcd(width, 512)
    final = pl.num_programs(0) - 1

    def piece(i, carry):
        at = pl.ds(pl.multiple_of(i * span, span), span)
        part = jnp.dot(hidden, down[0, :, at], preferred_element_type=F32)

        @pl.when(step == 0)
        def _():
            total[:, at] = part

        @pl.when((step > 0) & (step < final))
        def _():
            total[:, at] += part

        @pl.when(step == final)
        def _():
            out[:, at] = (total[:, at] + part).astype(BF)

        return carry

    lax.fori_loop(0, width // span, piece, 0)


def expert(rows, gate, up, down):
    count, width = rows.shape
    units = gate.shape[2]
    chunk = math.gcd(units // 2, 128)
    return pl.pallas_call(
        expert_body,
        grid=(units // chunk,),
        in_specs=[
            pl.BlockSpec((count, width), lambda i: (0, 0)),
            pl.BlockSpec((1, width, chunk), lambda i: (0, 0, i)),
            pl.BlockSpec((1, width, chunk), lambda i: (0, 0, i)),
            pl.BlockSpec((1, chunk, width), lambda i: (0, i, 0)),
        ],
        out_specs=pl.BlockSpec((count, width), lambda i: (0, 0)),
        out_shape=jax.ShapeDtypeStruct((count, width), BF),
        scratch_shapes=[pltpu.VMEM((count, width), F32)],
        compiler_params=params(60),
        name="expert",
    )(rows, gate, up, down)


def collect_body(returned, weights, resid, out):
    total = resid[...]
    for i in range(weights.shape[0]):
        total = total + jnp.dot(weights[i], returned[...], preferred_element_type=F32)
    out[...] = total.astype(BF)


def collect(returned, weights, resid):
    return pl.pallas_call(
        collect_body,
        out_shape=jax.ShapeDtypeStruct(resid.shape, BF),
        compiler_params=params(),
        name="collect",
    )(returned, weights, resid)


def three_pieces(value):
    pieces = []
    for _ in range(PIECES):
        piece = lax.reduce_precision(value, 8, 7)
        pieces.append(piece.astype(BF))
        value = value - piece
    return jnp.stack(pieces)


def shards(
    residual_in,
    query_small,
    query_large,
    key_small,
    key_large,
    value_small,
    value_large,
    forget_small,
    forget_large,
    project_small,
    project_large,
    norm_gain,
    expert_gate,
    expert_up,
    expert_down,
    routing,
    route_weight,
):
    head_devices = lax.axis_size("tp")
    experts = lax.axis_size("sp") * head_devices
    own_rows, width = residual_in.shape
    top_count = routing.shape[1]

    partial = attend_and_project(
        query_small,
        query_large,
        key_small,
        key_large,
        value_small,
        value_large,
        forget_small,
        forget_large,
        project_small,
        project_large,
    )

    capacity = max(2, 2 * own_rows * top_count // experts)
    pairs = own_rows * top_count
    pair_expert = routing.reshape(-1)
    same = pair_expert[:, None] == pair_expert[None, :]
    before = jnp.arange(pairs)[:, None] > jnp.arange(pairs)[None, :]
    slot = jnp.sum((same & before).astype(jnp.int32), axis=1)
    target = (pair_expert * capacity + slot).reshape(own_rows, top_count)
    hit = target[:, :, None] == jnp.arange(experts * capacity)[None, None, :]
    slots = jnp.any(hit, axis=1).T.astype(BF)
    weights = three_pieces(jnp.sum(jnp.where(hit, route_weight[:, :, None], 0.0), axis=1))

    parts = partial.reshape(head_devices, own_rows, width)
    parts = lax.all_to_all(parts, "tp", split_axis=0, concat_axis=0, tiled=True)
    resid, outgoing = mix(parts, residual_in, norm_gain.reshape(1, width), slots)
    outgoing = outgoing.reshape(experts, capacity, width)
    arrived = lax.all_to_all(outgoing, ("sp", "tp"), split_axis=0, concat_axis=0, tiled=True)
    result = expert(arrived.reshape(-1, width), expert_gate, expert_up, expert_down)
    result = result.reshape(experts, capacity, width)
    returned = lax.all_to_all(result, ("sp", "tp"), split_axis=0, concat_axis=0, tiled=True)
    return collect(returned.reshape(-1, width), weights, resid)


def solution(mesh):
    in_specs = (
        P(("grp", "sp", "tp"), None),
        P(("grp", "sp"), "tp"),
        P(("grp", "sp"), "tp"),
        P(None, ("grp", "sp")),
        P(None, ("grp", "sp")),
        P(None, ("grp", "sp")),
        P(None, ("grp", "sp")),
        P("tp", ("grp", "sp")),
        P("tp", ("grp", "sp")),
        P("tp", None),
        P("tp", None),
        P(),
        P(("sp", "tp"), None, None),
        P(("sp", "tp"), None, None),
        P(("sp", "tp"), None, None),
        P(("grp", "sp", "tp"), None),
        P(("grp", "sp", "tp"), None),
    )
    out_specs = P(("grp", "sp", "tp"), None)

    return jax.shard_map(shards, mesh=mesh, in_specs=in_specs, out_specs=out_specs, check_vma=False)
```

profile of v0, /device:TPU:33, one launch (start us, length us, event | category | flops | bytes accessed | tf_op | source)
XLA Modules:
  0.0 282.2 jit_solution(5409717616663720416)
XLA Ops:
  1.6 20.5 %collective-permute-start.10 = (bf16[416,256]{1,0:T(8,128)(2,1)S(1)}, bf16[416,256]{1,0:T(8,128)(2,1)S(1)}, u32[]{:S(2)}, u32[]{:S(2)}) collective-permute-start(bf16[416,256]{1,0:T(8,128)(2,1)S(1)} %packed.1.block), channel_id=1, source_target_pairs={{0,4},{4,0},{8,12},{12,8},{16,20},{20,16},{24,28},{28,24},{32,36},... | collective-permute-start | bytes 638984 | tf_op jit(solution)/shard_map/ppermute | solution.py:242
  22.2 3.1 %collective-permute-start.2 = (bf16[416,256]{1,0:T(8,128)(2,1)S(1)}, bf16[416,256]{1,0:T(8,128)(2,1)S(1)}, u32[]{:S(2)}, u32[]{:S(2)}) collective-permute-start(bf16[416,256]{1,0:T(8,128)(2,1)S(1)} %packed.1.block), channel_id=1, source_target_pairs={{0,8},{4,124},{8,16},{12,4},{16,24},{20,12},{24,32},{28,20},{32,40... | collective-permute-start | bytes 638984 | tf_op jit(solution)/shard_map/ppermute | solution.py:247
  28.1 3.1 %collective-permute-start.3 = (bf16[416,256]{1,0:T(8,128)(2,1)S(1)}, bf16[416,256]{1,0:T(8,128)(2,1)S(1)}, u32[]{:S(2)}, u32[]{:S(2)}) collective-permute-start(bf16[416,256]{1,0:T(8,128)(2,1)S(1)} %collective-permute-done.2.refs_0_), channel_id=1, source_target_pairs={{0,8},{4,124},{8,16},{12,4},{16,24},{20,12},{24,32},{28,20},{32,40... | collective-permute-start | bytes 638984 | tf_op jit(solution)/shard_map/ppermute | solution.py:247
  31.2 2.3 collective-permute-start.12
  34.0 3.1 %collective-permute-start.4 = (bf16[416,256]{1,0:T(8,128)(2,1)S(1)}, bf16[416,256]{1,0:T(8,128)(2,1)S(1)}, u32[]{:S(2)}, u32[]{:S(2)}) collective-permute-start(bf16[416,256]{1,0:T(8,128)(2,1)S(1)} %collective-permute-done.3.refs_0_), channel_id=1, source_target_pairs={{0,8},{4,124},{8,16},{12,4},{16,24},{20,12},{24,32},{28,20},{32,40... | collective-permute-start | bytes 638984 | tf_op jit(solution)/shard_map/ppermute | solution.py:247
  37.1 2.3 collective-permute-start.13
  39.9 3.1 %collective-permute-start.5 = (bf16[416,256]{1,0:T(8,128)(2,1)S(1)}, bf16[416,256]{1,0:T(8,128)(2,1)S(1)}, u32[]{:S(2)}, u32[]{:S(2)}) collective-permute-start(bf16[416,256]{1,0:T(8,128)(2,1)S(1)} %collective-permute-done.4.refs_0_), channel_id=1, source_target_pairs={{0,8},{4,124},{8,16},{12,4},{16,24},{20,12},{24,32},{28,20},{32,40... | collective-permute-start | bytes 638984 | tf_op jit(solution)/shard_map/ppermute | solution.py:247
  43.0 2.3 collective-permute-start.14
  45.8 3.1 %collective-permute-start.6 = (bf16[416,256]{1,0:T(8,128)(2,1)S(1)}, bf16[416,256]{1,0:T(8,128)(2,1)S(1)}, u32[]{:S(2)}, u32[]{:S(2)}) collective-permute-start(bf16[416,256]{1,0:T(8,128)(2,1)S(1)} %collective-permute-done.5.refs_0_), channel_id=1, source_target_pairs={{0,8},{4,124},{8,16},{12,4},{16,24},{20,12},{24,32},{28,20},{32,40... | collective-permute-start | bytes 638984 | tf_op jit(solution)/shard_map/ppermute | solution.py:247
  48.9 2.3 collective-permute-start.15
  51.7 3.1 %collective-permute-start.7 = (bf16[416,256]{1,0:T(8,128)(2,1)S(1)}, bf16[416,256]{1,0:T(8,128)(2,1)S(1)}, u32[]{:S(2)}, u32[]{:S(2)}) collective-permute-start(bf16[416,256]{1,0:T(8,128)(2,1)S(1)} %collective-permute-done.6.refs_0_), channel_id=1, source_target_pairs={{0,8},{4,124},{8,16},{12,4},{16,24},{20,12},{24,32},{28,20},{32,40... | collective-permute-start | bytes 638984 | tf_op jit(solution)/shard_map/ppermute | solution.py:247
  54.8 2.3 collective-permute-start.16
  57.6 3.1 %collective-permute-start.8 = (bf16[416,256]{1,0:T(8,128)(2,1)S(1)}, bf16[416,256]{1,0:T(8,128)(2,1)S(1)}, u32[]{:S(2)}, u32[]{:S(2)}) collective-permute-start(bf16[416,256]{1,0:T(8,128)(2,1)S(1)} %collective-permute-done.7.refs_0_), channel_id=1, source_target_pairs={{0,8},{4,124},{8,16},{12,4},{16,24},{20,12},{24,32},{28,20},{32,40... | collective-permute-start | bytes 638984 | tf_op jit(solution)/shard_map/ppermute | solution.py:247
  60.7 4.1 %collective-permute-start = (bf16[256,256]{1,0:T(8,128)(2,1)}, bf16[256,256]{1,0:T(8,128)(2,1)S(1)}, u32[]{:S(2)}, u32[]{:S(2)}) collective-permute-start(bf16[256,256]{1,0:T(8,128)(2,1)} %own_s.1), channel_id=1, source_target_pairs={{0,4},{4,0},{8,12},{12,8},{16,20},{20,16},{24,28},{28,24},{32,36},... | collective-permute-start | bytes 393224 | tf_op jit(solution)/shard_map/ppermute | solution.py:237
  64.8 3.0 %collective-permute-start.17 = (bf16[416,256]{1,0:T(8,128)(2,1)S(1)}, bf16[416,256]{1,0:T(8,128)(2,1)S(1)}, u32[]{:S(2)}, u32[]{:S(2)}) collective-permute-start(bf16[416,256]{1,0:T(8,128)(2,1)S(1)} %collective-permute-done.16.refs_1_), channel_id=1, source_target_pairs={{0,8},{4,124},{8,16},{12,4},{16,24},{20,12},{24,32},{28,20},{32,40... | collective-permute-start | bytes 638984 | tf_op jit(solution)/shard_map/ppermute | solution.py:250
  69.8 3.7 %first.1 = (bf16[4,80,256]{2,1,0:T(8,128)(2,1)S(1)}, bf16[2,144,256]{2,1,0:T(8,128)(2,1)S(1)}, bf16[4,80,256]{2,1,0:T(8,128)(2,1)S(1)}, bf16[2,144,256]{2,1,0:T(...) custom-call(s32[9]{0:T(128)S(1)} %pad_add_fusion.info.flags, ...), custom_call_target="tpu_custom_call" | custom-call | tf_op jit(solution)/shard_map/first/pallas_call | solution.py:162
  78.1 6.4 %collective-permute-start.18 = (f32[4,88,256]{2,1,0:T(8,128)S(1)}, f32[4,88,256]{2,1,0:T(8,128)S(1)}, u32[]{:S(2)}, u32[]{:S(2)}) collective-permute-start(f32[4,88,256]{2,1,0:T(8,128)S(1)} %get-tuple-element.85), channel_id=1, source_target_pairs={{0,4},{4,0},{8,12},{12,8},{16,20},{20,16},{24,28},{28,24},{32,36},... | collective-permute-start | bytes 1081352 | tf_op jit(solution)/shard_map/ppermute | solution.py:253
  88.0 4.4 %all-to-all-start = ((bf16[4,64,2048]{2,1,0:T(8,128)(2,1)}), bf16[4,64,2048]{2,1,0:T(8,128)(2,1)S(1)}, u32[]{:S(2)}, u32[]{:S(2)}) async-start(bf16[4,64,2048]{2,1,0:T(8,128)(2,1)} %bitcast.1), calls=%async_computation | async-start | bytes 2097152 | tf_op jit(solution)/shard_map/all_to_all | solution.py:407
  93.4 13.6 %all-to-all-done.parts = bf16[4,64,2048]{2,1,0:T(8,128)(2,1)S(1)} async-done(((bf16[4,64,2048]{2,1,0:T(8,128)(2,1)}), bf16[4,64,2048]{2,1,0:T(8,128)(2,1)S(1)}, u32[]{:S(2)}, u32[]{:S(2)}) %all-to-all-start) | async-done | bytes 1048608 | tf_op jit(solution)/shard_map/all_to_all | solution.py:407
  108.4 94.4 %all_to_all.15 = bf16[128,2,2048]{2,1,0:T(2,128)(2,1)S(1)} all-to-all(bf16[128,2,2048]{2,1,0:T(2,128)(2,1)S(1)} %reshape.70), channel_id=1, replica_groups=mesh['grp'=2,'sp'=32,'tp'=4] {'sp','tp'}, dimensions={0} | all-to-all | bytes 2097152 | tf_op jit(solution)/shard_map/all_to_all | solution.py:410
  204.0 10.0 %expert.1 = bf16[256,2048]{1,0:T(8,128)(2,1)} custom-call(bf16[256,2048]{1,0:T(8,128)(2,1)} %reshape.71.rows, bf16[1,2048,512]{2,1,0:T(8,128)(2,1)} %gate.1, bf16[1,2048,512]{2,1,0:T(8,128)(2,1)} %up.1, bf16[1,512,2048]{2,1,0:T(8,128)(2,1)} %down.1), custom_call_target="tpu_custom_call" | custom-call | tf_op jit(solution)/shard_map/expert/pallas_call | solution.py:316
  214.0 2.5 reshape.72
  216.5 8.5 %all-to-all-start.2 = ((bf16[128,2,2048]{2,1,0:T(2,128)(2,1)}), bf16[128,2,2048]{2,1,0:T(2,128)(2,1)}, u32[]{:S(2)}, u32[]{:S(2)}) async-start(bf16[128,2,2048]{2,1,0:T(2,128)(2,1)} %reshape.72), calls=%async_computation.2 | async-start | bytes 2097152 | tf_op jit(solution)/shard_map/all_to_all | solution.py:413
  225.2 54.2 %all-to-all-done.2 = bf16[128,2,2048]{2,1,0:T(2,128)(2,1)} async-done(((bf16[128,2,2048]{2,1,0:T(2,128)(2,1)}), bf16[128,2,2048]{2,1,0:T(2,128)(2,1)}, u32[]{:S(2)}, u32[]{:S(2)}) %all-to-all-start.2) | async-done | bytes 1048608 | tf_op jit(solution)/shard_map/all_to_all | solution.py:413
  (72 shorter events, 23.4 us)
Async XLA Ops:
  1.6 23.6 %collective-permute-start.10 = (bf16[416,256]{1,0:T(8,128)(2,1)S(1)}, bf16[416,256]{1,0:T(8,128)(2,1)S(1)}, u32[]{:S(2)}, u32[]{:S(2)}) collective-permute-start(bf16[416,256]{1,0:T(8,128)(2,1)S(1)} %packed.1.block), channel_id=1, source_target_pairs={{0,4},{4,0},{8,12},{12,8},{16,20},{20,16},{24,28},{28,24},{32,36},... | collective-permute-start | bytes 638984 | tf_op jit(solution)/shard_map/ppermute | solution.py:242
  22.2 5.9 %collective-permute-start.2 = (bf16[416,256]{1,0:T(8,128)(2,1)S(1)}, bf16[416,256]{1,0:T(8,128)(2,1)S(1)}, u32[]{:S(2)}, u32[]{:S(2)}) collective-permute-start(bf16[416,256]{1,0:T(8,128)(2,1)S(1)} %packed.1.block), channel_id=1, source_target_pairs={{0,8},{4,124},{8,16},{12,4},{16,24},{20,12},{24,32},{28,20},{32,40... | collective-permute-start | bytes 638984 | tf_op jit(solution)/shard_map/ppermute | solution.py:247
  25.3 5.9 %collective-permute-start.11 = (bf16[416,256]{1,0:T(8,128)(2,1)S(1)}, bf16[416,256]{1,0:T(8,128)(2,1)S(1)}, u32[]{:S(2)}, u32[]{:S(2)}) collective-permute-start(bf16[416,256]{1,0:T(8,128)(2,1)S(1)} %collective-permute-done.10), channel_id=1, source_target_pairs={{0,8},{4,124},{8,16},{12,4},{16,24},{20,12},{24,32},{28,20},{32,40... | collective-permute-start | bytes 638984 | tf_op jit(solution)/shard_map/ppermute | solution.py:250
  28.1 5.9 %collective-permute-start.3 = (bf16[416,256]{1,0:T(8,128)(2,1)S(1)}, bf16[416,256]{1,0:T(8,128)(2,1)S(1)}, u32[]{:S(2)}, u32[]{:S(2)}) collective-permute-start(bf16[416,256]{1,0:T(8,128)(2,1)S(1)} %collective-permute-done.2.refs_0_), channel_id=1, source_target_pairs={{0,8},{4,124},{8,16},{12,4},{16,24},{20,12},{24,32},{28,20},{32,40... | collective-permute-start | bytes 638984 | tf_op jit(solution)/shard_map/ppermute | solution.py:247
  31.2 5.9 %collective-permute-start.12 = (bf16[416,256]{1,0:T(8,128)(2,1)S(1)}, bf16[416,256]{1,0:T(8,128)(2,1)S(1)}, u32[]{:S(2)}, u32[]{:S(2)}) collective-permute-start(bf16[416,256]{1,0:T(8,128)(2,1)S(1)} %collective-permute-done.11.refs_1_), channel_id=1, source_target_pairs={{0,8},{4,124},{8,16},{12,4},{16,24},{20,12},{24,32},{28,20},{32,40... | collective-permute-start | bytes 638984 | tf_op jit(solution)/shard_map/ppermute | solution.py:250
  34.0 5.9 %collective-permute-start.4 = (bf16[416,256]{1,0:T(8,128)(2,1)S(1)}, bf16[416,256]{1,0:T(8,128)(2,1)S(1)}, u32[]{:S(2)}, u32[]{:S(2)}) collective-permute-start(bf16[416,256]{1,0:T(8,128)(2,1)S(1)} %collective-permute-done.3.refs_0_), channel_id=1, source_target_pairs={{0,8},{4,124},{8,16},{12,4},{16,24},{20,12},{24,32},{28,20},{32,40... | collective-permute-start | bytes 638984 | tf_op jit(solution)/shard_map/ppermute | solution.py:247
  37.1 5.9 %collective-permute-start.13 = (bf16[416,256]{1,0:T(8,128)(2,1)S(1)}, bf16[416,256]{1,0:T(8,128)(2,1)S(1)}, u32[]{:S(2)}, u32[]{:S(2)}) collective-permute-start(bf16[416,256]{1,0:T(8,128)(2,1)S(1)} %collective-permute-done.12.refs_1_), channel_id=1, source_target_pairs={{0,8},{4,124},{8,16},{12,4},{16,24},{20,12},{24,32},{28,20},{32,40... | collective-permute-start | bytes 638984 | tf_op jit(solution)/shard_map/ppermute | solution.py:250
  39.9 5.9 %collective-permute-start.5 = (bf16[416,256]{1,0:T(8,128)(2,1)S(1)}, bf16[416,256]{1,0:T(8,128)(2,1)S(1)}, u32[]{:S(2)}, u32[]{:S(2)}) collective-permute-start(bf16[416,256]{1,0:T(8,128)(2,1)S(1)} %collective-permute-done.4.refs_0_), channel_id=1, source_target_pairs={{0,8},{4,124},{8,16},{12,4},{16,24},{20,12},{24,32},{28,20},{32,40... | collective-permute-start | bytes 638984 | tf_op jit(solution)/shard_map/ppermute | solution.py:247
  43.0 5.9 %collective-permute-start.14 = (bf16[416,256]{1,0:T(8,128)(2,1)S(1)}, bf16[416,256]{1,0:T(8,128)(2,1)S(1)}, u32[]{:S(2)}, u32[]{:S(2)}) collective-permute-start(bf16[416,256]{1,0:T(8,128)(2,1)S(1)} %collective-permute-done.13.refs_1_), channel_id=1, source_target_pairs={{0,8},{4,124},{8,16},{12,4},{16,24},{20,12},{24,32},{28,20},{32,40... | collective-permute-start | bytes 638984 | tf_op jit(solution)/shard_map/ppermute | solution.py:250
  45.8 5.9 %collective-permute-start.6 = (bf16[416,256]{1,0:T(8,128)(2,1)S(1)}, bf16[416,256]{1,0:T(8,128)(2,1)S(1)}, u32[]{:S(2)}, u32[]{:S(2)}) collective-permute-start(bf16[416,256]{1,0:T(8,128)(2,1)S(1)} %collective-permute-done.5.refs_0_), channel_id=1, source_target_pairs={{0,8},{4,124},{8,16},{12,4},{16,24},{20,12},{24,32},{28,20},{32,40... | collective-permute-start | bytes 638984 | tf_op jit(solution)/shard_map/ppermute | solution.py:247
  48.9 5.9 %collective-permute-start.15 = (bf16[416,256]{1,0:T(8,128)(2,1)S(1)}, bf16[416,256]{1,0:T(8,128)(2,1)S(1)}, u32[]{:S(2)}, u32[]{:S(2)}) collective-permute-start(bf16[416,256]{1,0:T(8,128)(2,1)S(1)} %collective-permute-done.14.refs_1_), channel_id=1, source_target_pairs={{0,8},{4,124},{8,16},{12,4},{16,24},{20,12},{24,32},{28,20},{32,40... | collective-permute-start | bytes 638984 | tf_op jit(solution)/shard_map/ppermute | solution.py:250
  51.7 5.9 %collective-permute-start.7 = (bf16[416,256]{1,0:T(8,128)(2,1)S(1)}, bf16[416,256]{1,0:T(8,128)(2,1)S(1)}, u32[]{:S(2)}, u32[]{:S(2)}) collective-permute-start(bf16[416,256]{1,0:T(8,128)(2,1)S(1)} %collective-permute-done.6.refs_0_), channel_id=1, source_target_pairs={{0,8},{4,124},{8,16},{12,4},{16,24},{20,12},{24,32},{28,20},{32,40... | collective-permute-start | bytes 638984 | tf_op jit(solution)/shard_map/ppermute | solution.py:247
  54.8 10.0 %collective-permute-start.16 = (bf16[416,256]{1,0:T(8,128)(2,1)S(1)}, bf16[416,256]{1,0:T(8,128)(2,1)S(1)}, u32[]{:S(2)}, u32[]{:S(2)}) collective-permute-start(bf16[416,256]{1,0:T(8,128)(2,1)S(1)} %collective-permute-done.15.refs_1_), channel_id=1, source_target_pairs={{0,8},{4,124},{8,16},{12,4},{16,24},{20,12},{24,32},{28,20},{32,40... | collective-permute-start | bytes 638984 | tf_op jit(solution)/shard_map/ppermute | solution.py:250
  57.6 10.2 %collective-permute-start.8 = (bf16[416,256]{1,0:T(8,128)(2,1)S(1)}, bf16[416,256]{1,0:T(8,128)(2,1)S(1)}, u32[]{:S(2)}, u32[]{:S(2)}) collective-permute-start(bf16[416,256]{1,0:T(8,128)(2,1)S(1)} %collective-permute-done.7.refs_0_), channel_id=1, source_target_pairs={{0,8},{4,124},{8,16},{12,4},{16,24},{20,12},{24,32},{28,20},{32,40... | collective-permute-start | bytes 638984 | tf_op jit(solution)/shard_map/ppermute | solution.py:247
  60.7 7.3 %collective-permute-start = (bf16[256,256]{1,0:T(8,128)(2,1)}, bf16[256,256]{1,0:T(8,128)(2,1)S(1)}, u32[]{:S(2)}, u32[]{:S(2)}) collective-permute-start(bf16[256,256]{1,0:T(8,128)(2,1)} %own_s.1), channel_id=1, source_target_pairs={{0,4},{4,0},{8,12},{12,8},{16,20},{20,16},{24,28},{28,24},{32,36},... | collective-permute-start | bytes 393224 | tf_op jit(solution)/shard_map/ppermute | solution.py:237
  64.8 3.2 %collective-permute-start.1 = (bf16[256,256]{1,0:T(8,128)(2,1)}, bf16[256,256]{1,0:T(8,128)(2,1)}, u32[]{:S(2)}, u32[]{:S(2)}) collective-permute-start(bf16[256,256]{1,0:T(8,128)(2,1)} %own_l.1), channel_id=1, source_target_pairs={{0,4},{4,0},{8,12},{12,8},{16,20},{20,16},{24,28},{28,24},{32,36},... | collective-permute-start | bytes 393224 | tf_op jit(solution)/shard_map/ppermute | solution.py:238
  64.8 12.1 %collective-permute-start.17 = (bf16[416,256]{1,0:T(8,128)(2,1)S(1)}, bf16[416,256]{1,0:T(8,128)(2,1)S(1)}, u32[]{:S(2)}, u32[]{:S(2)}) collective-permute-start(bf16[416,256]{1,0:T(8,128)(2,1)S(1)} %collective-permute-done.16.refs_1_), channel_id=1, source_target_pairs={{0,8},{4,124},{8,16},{12,4},{16,24},{20,12},{24,32},{28,20},{32,40... | collective-permute-start | bytes 638984 | tf_op jit(solution)/shard_map/ppermute | solution.py:250
  67.8 9.7 %collective-permute-start.9 = (bf16[416,256]{1,0:T(8,128)(2,1)S(1)}, bf16[416,256]{1,0:T(8,128)(2,1)S(1)}, u32[]{:S(2)}, u32[]{:S(2)}) collective-permute-start(bf16[416,256]{1,0:T(8,128)(2,1)S(1)} %collective-permute-done.8.refs_0_), channel_id=1, source_target_pairs={{0,8},{4,124},{8,16},{12,4},{16,24},{20,12},{24,32},{28,20},{32,40... | collective-permute-start | bytes 638984 | tf_op jit(solution)/shard_map/ppermute | solution.py:247
  78.1 8.2 %collective-permute-start.18 = (f32[4,88,256]{2,1,0:T(8,128)S(1)}, f32[4,88,256]{2,1,0:T(8,128)S(1)}, u32[]{:S(2)}, u32[]{:S(2)}) collective-permute-start(f32[4,88,256]{2,1,0:T(8,128)S(1)} %get-tuple-element.85), channel_id=1, source_target_pairs={{0,4},{4,0},{8,12},{12,8},{16,20},{20,16},{24,28},{28,24},{32,36},... | collective-permute-start | bytes 1081352 | tf_op jit(solution)/shard_map/ppermute | solution.py:253
  84.5 1.7 collective-permute-start.19
  88.0 19.0 %copy-start.2 = (bf16[64,2048]{1,0:T(8,128)(2,1)S(1)}, bf16[64,2048]{1,0:T(8,128)(2,1)}, u32[]{:S(2)}) copy-start(bf16[64,2048]{1,0:T(8,128)(2,1)} %residual_in.1) | copy-start | bytes 786436
  88.0 19.0 %all-to-all-start = ((bf16[4,64,2048]{2,1,0:T(8,128)(2,1)}), bf16[4,64,2048]{2,1,0:T(8,128)(2,1)S(1)}, u32[]{:S(2)}, u32[]{:S(2)}) async-start(bf16[4,64,2048]{2,1,0:T(8,128)(2,1)} %bitcast.1), calls=%async_computation | async-start | bytes 2097152 | tf_op jit(solution)/shard_map/all_to_all | solution.py:407
  214.0 11.0 %copy-start.7 = (f32[64,2]{0,1:T(2,128)S(1)}, f32[64,2]{0,1:T(2,128)}, u32[]{:S(2)}) copy-start(f32[64,2]{0,1:T(2,128)} %param.33) | copy-start | bytes 1540
  216.5 62.9 %all-to-all-start.2 = ((bf16[128,2,2048]{2,1,0:T(2,128)(2,1)}), bf16[128,2,2048]{2,1,0:T(2,128)(2,1)}, u32[]{:S(2)}, u32[]{:S(2)}) async-start(bf16[128,2,2048]{2,1,0:T(2,128)(2,1)} %reshape.72), calls=%async_computation.2 | async-start | bytes 2097152 | tf_op jit(solution)/shard_map/all_to_all | solution.py:413
  (6 other events, 30.3 us)
where the time goes:
time: 283 us; the launch traced here: 282 us
  blocking collectives  94.4 us (33%)
  starting transfers between devices  81.5 us (29%)
  waiting for transfers between devices  73.7 us (26%)
  Pallas kernels  21.9 us (8%)
  local copies, waits for them, and re-layouts  8.3 us (3%)
    all_to_all x1, blocking collectives, shards(): lax.all_to_all(outgoing, ('sp', 'tp'), split_axis=0, concat_axis=0, tiled...  94.4 us
    all_to_all x1, waiting for transfers between devices, shards(): lax.all_to_all(result, ('sp', 'tp'), split_axis=0, concat_axis=0, tiled=T...  54.2 us
    ppermute x8, starting transfers between devices, attend_and_project(): a = lax.ppermute(a, 'sp', ring)  21.9 us
    ppermute x1, starting transfers between devices, attend_and_project(): b = lax.ppermute(block, 'sp', swap)  20.5 us
    ppermute x7, starting transfers between devices, attend_and_project(): b = lax.ppermute(b, 'sp', ring)  15.4 us
    all_to_all x1, waiting for transfers between devices, shards(): parts = lax.all_to_all(parts, 'tp', split_axis=0, concat_axis=0, tiled=True)  13.6 us
    pallas_call x1, Pallas kernels, expert(): pl.pallas_call(expert_body, grid=(units // chunk,), in_specs=[pl.BlockSpe...  9.96 us
    all_to_all x1, starting transfers between devices, shards(): lax.all_to_all(result, ('sp', 'tp'), split_axis=0, concat_axis=0, tiled=T...  8.49 us
  transfers between devices with their start and end apart: 22, of which 9 were waited for; matrix products, arithmetic and copies ran while one was open for 0% of the time, Pallas kernels for 3%

commit v1 on v0

--- a/solution.py
+++ b/solution.py
@@ -1,3 +1,4 @@
+import functools
 import math
 
 import jax
@@ -72,15 +73,22 @@
         s = following
 
 
-def lay_out(blocks, ks, vs, kl, vl):
+def lay_out(blocks, ks, vs, kl, vl, usable=None):
     size_s, size_l = ks.shape[1] - GATE_ROWS, kl.shape[1] - GATE_ROWS
     a = size_s + GATE_ROWS
     b = a + size_l + GATE_ROWS
     for i, block in enumerate(blocks):
         count = block.shape[1]
         at = pl.ds(i * count, count)
-        ks[at] = block[0:a].T
-        kl[at] = block[a:b].T
+
+        def with_gates(first, size):
+            gates = block[first + size : first + size + GATE_ROWS]
+            if usable is not None:
+                gates = jnp.where(usable[i] == 1, gates.astype(F32), LOW).astype(BF)
+            return jnp.concatenate([block[first : first + size], gates], axis=0).T
+
+        ks[at] = with_gates(0, size_s)
+        kl[at] = with_gates(a, size_l)
         vs[:size_s, at] = block[b : b + size_s]
         vl[:size_l, at] = block[b + size_s :]
     vs[size_s:] = jnp.ones((GATE_ROWS, vs.shape[1]), BF)
@@ -170,13 +178,15 @@
     )(info, own_s, own_l, peer_s, peer_l, block)
 
 
-def advance(info, step, queries, blocks, states):
+def advance(info, steps, queries, blocks, states):
     def body(flags, qs_o, ql_o, qs_p, ql_p, *refs):
         arrived, (ss_o, sl_o, ss_p, sl_p), laid = refs[: len(blocks)], refs[-8:-4], refs[-4:]
-
-        @pl.when(flags[step] == 1)
+        usable = [flags[step] for step in steps]
+        some = functools.reduce(jnp.maximum, usable)
+
+        @pl.when(some == 1)
         def _():
-            lay_out(arrived, *laid)
+            lay_out(arrived, *laid, usable=usable)
             add_keys([(qs_o, ql_o, ss_o, sl_o), (qs_p, ql_p, ss_p, sl_p)], *laid)
 
     vm = pl.BlockSpec(memory_space=pltpu.VMEM)
@@ -243,16 +253,25 @@
     a = block
     made = first(info, qs, ql, peer_s, peer_l, block, gs.shape[0], gl.shape[0])
     queries, states = made[:4], made[4:]
+    waiting, at = [], []
     for step in range(1, steps + 1):
         a = lax.ppermute(a, "sp", ring)
-        blocks = [a]
+        waiting.append(a)
+        at.append(step)
         if step < steps or chips % 2:
             b = lax.ppermute(b, "sp", ring)
-            blocks.append(b)
-        states = advance(info, step, queries, blocks, states)
+            waiting.append(b)
+            at.append(step)
+        if worked_at(step, steps):
+            states = advance(info, at, queries, waiting, states)
+            waiting, at = [], []
     got_s = lax.ppermute(states[2], "sp", swap)
     got_l = lax.ppermute(states[3], "sp", swap)
     return finish(states[0], states[1], got_s, got_l, ps, pb)
+
+
+def worked_at(step, steps):
+    return step % 2 == 1 or step == steps
 
 
 def mix_body(parts, residual_in, gain, slots, resid_out, outgoing):
@@ -279,53 +298,64 @@
     )(parts, residual_in, gain, slots)
 
 
-def expert_body(rows, gate, up, down, out, total):
-    step = pl.program_id(0)
-    g = jnp.dot(rows[...], gate[0], preferred_element_type=F32)
-    u = jnp.dot(rows[...], up[0], preferred_element_type=F32)
-    hidden = (g / (1.0 + jnp.exp(-g)) * u).astype(BF)
-    width = out.shape[1]
-    span = math.gcd(width, 512)
-    final = pl.num_programs(0) - 1
-
-    def piece(i, carry):
-        at = pl.ds(pl.multiple_of(i * span, span), span)
-        part = jnp.dot(hidden, down[0, :, at], preferred_element_type=F32)
-
-        @pl.when(step == 0)
-        def _():
-            total[:, at] = part
-
-        @pl.when((step > 0) & (step < final))
-        def _():
-            total[:, at] += part
-
-        @pl.when(step == final)
-        def _():
-            out[:, at] = (total[:, at] + part).astype(BF)
-
-        return carry
-
-    lax.fori_loop(0, width // span, piece, 0)
-
-
 def expert(rows, gate, up, down):
     count, width = rows.shape
     units = gate.shape[2]
-    chunk = math.gcd(units // 2, 128)
-    return pl.pallas_call(
-        expert_body,
-        grid=(units // chunk,),
-        in_specs=[
-            pl.BlockSpec((count, width), lambda i: (0, 0)),
-            pl.BlockSpec((1, width, chunk), lambda i: (0, 0, i)),
-            pl.BlockSpec((1, width, chunk), lambda i: (0, 0, i)),
-            pl.BlockSpec((1, chunk, width), lambda i: (0, i, 0)),
+    pieces = 4
+    deep = width // pieces
+    span = math.gcd(width, 512)
+
+    def body(rows, gate, up, down, out, gate_v, up_v, down_v, g, u, hidden, sems):
+        def inward(i):
+            at = pl.ds(pl.multiple_of(i * deep, deep), deep)
+            return (
+                pltpu.make_async_copy(gate.at[0, at], gate_v.at[at], sems.at[2 * i]),
+                pltpu.make_async_copy(up.at[0, at], up_v.at[at], sems.at[2 * i + 1]),
+            )
+
+        outward = pltpu.make_async_copy(down.at[0], down_v, sems.at[2 * pieces])
+        for i in range(pieces):
+            for copy in inward(i):
+                copy.start()
+        outward.start()
+        g[...] = jnp.zeros_like(g)
+        u[...] = jnp.zeros_like(u)
+
+        def first_products(i, carry):
+            at = pl.ds(pl.multiple_of(i * deep, deep), deep)
+            for copy, weight, total in zip(inward(i), (gate_v, up_v), (g, u)):
+                copy.wait()
+                total[...] += jnp.dot(rows[:, at], weight[at], preferred_element_type=F32)
+            return carry
+
+        lax.fori_loop(0, pieces, first_products, 0)
+        gated = g[...]
+        hidden[...] = (gated / (1.0 + jnp.exp(-gated)) * u[...]).astype(BF)
+        outward.wait()
+
+        def last_product(i, carry):
+            at = pl.ds(pl.multiple_of(i * span, span), span)
+            out[:, at] = jnp.dot(hidden[...], down_v[:, at], preferred_element_type=F32).astype(BF)
+            return carry
+
+        lax.fori_loop(0, width // span, last_product, 0)
+
+    vm = pl.BlockSpec(memory_space=pltpu.VMEM)
+    return pl.pallas_call(
+        body,
+        in_specs=[vm] + [pl.BlockSpec(memory_space=pltpu.HBM)] * 3,
+        out_specs=vm,
+        out_shape=jax.ShapeDtypeStruct((count, width), BF),
+        scratch_shapes=[
+            pltpu.VMEM((width, units), BF),
+            pltpu.VMEM((width, units), BF),
+            pltpu.VMEM((units, width), BF),
+            pltpu.VMEM((count, units), F32),
+            pltpu.VMEM((count, units), F32),
+            pltpu.VMEM((count, units), BF),
+            pltpu.SemaphoreType.DMA((2 * pieces + 1,)),
         ],
-        out_specs=pl.BlockSpec((count, width), lambda i: (0, 0)),
-        out_shape=jax.ShapeDtypeStruct((count, width), BF),
-        scratch_shapes=[pltpu.VMEM((count, width), F32)],
-        compiler_params=params(60),
+        compiler_params=params(57),
         name="expert",
     )(rows, gate, up, down)
 

time: 283 us -> 275 us (0.972)
  Pallas kernels: 21.9 us -> 17.4 us
  blocking collectives: 94.4 us -> 91.4 us
    all_to_all x1, blocking collectives: 94.4 us -> 91.4 us  [shards(): lax.all_to_all(outgoing, ('sp', 'tp'), split_axis=0, concat_axis=0, tiled...]
    pallas_call x1, Pallas kernels: 9.96 us -> 7.12 us  [expert(): pl.pallas_call(body, in_specs=[vm] + [pl.BlockSpec(memory_space=pltpu.HBM...]
  transfers between devices with their start and end apart: 22 -> 22, of which waited for: 9 -> 9; matrix products, arithmetic and copies ran while one was open for 0% -> 0% of each run, Pallas kernels for 3% -> 2%
where the time goes in v1:
time: 275 us
  blocking collectives  91.4 us (33%)
  starting transfers between devices  81.5 us (30%)
  waiting for transfers between devices  73.7 us (27%)
  Pallas kernels  17.4 us (6%)
  local copies, waits for them, and re-layouts  8.32 us (3%)
    all_to_all x1, blocking collectives, shards(): lax.all_to_all(outgoing, ('sp', 'tp'), split_axis=0, concat_axis=0, tiled...  91.4 us
    all_to_all x1, waiting for transfers between devices, shards(): lax.all_to_all(result, ('sp', 'tp'), split_axis=0, concat_axis=0, tiled=T...  54.2 us
    ppermute x8, starting transfers between devices, attend_and_project(): a = lax.ppermute(a, 'sp', ring)  21.9 us
    ppermute x1, starting transfers between devices, attend_and_project(): b = lax.ppermute(block, 'sp', swap)  20.5 us
    ppermute x7, starting transfers between devices, attend_and_project(): b = lax.ppermute(b, 'sp', ring)  15.4 us
    all_to_all x1, waiting for transfers between devices, shards(): parts = lax.all_to_all(parts, 'tp', split_axis=0, concat_axis=0, tiled=True)  13.6 us
    all_to_all x1, starting transfers between devices, shards(): lax.all_to_all(result, ('sp', 'tp'), split_axis=0, concat_axis=0, tiled=T...  8.49 us
    pallas_call x1, Pallas kernels, expert(): pl.pallas_call(body, in_specs=[vm] + [pl.BlockSpec(memory_space=pltpu.HBM...  7.12 us
  transfers between devices with their start and end apart: 22, of which 9 were waited for; matrix products, arithmetic and copies ran while one was open for 0% of the time, Pallas kernels for 2%

profile of v1, /device:TPU:33, one launch (start us, length us, event | category | flops | bytes accessed | tf_op | source)
XLA Modules:
  0.0 274.7 jit_solution(9515087633630028221)
XLA Ops:
  1.6 20.5 %collective-permute-start.10 = (bf16[416,256]{1,0:T(8,128)(2,1)S(1)}, bf16[416,256]{1,0:T(8,128)(2,1)S(1)}, u32[]{:S(2)}, u32[]{:S(2)}) collective-permute-start(bf16[416,256]{1,0:T(8,128)(2,1)S(1)} %packed.1.block), channel_id=1, source_target_pairs={{0,4},{4,0},{8,12},{12,8},{16,20},{20,16},{24,28},{28,24},{32,36},... | collective-permute-start | bytes 638984 | tf_op jit(solution)/shard_map/ppermute | solution.py:252
  22.2 3.1 %collective-permute-start.2 = (bf16[416,256]{1,0:T(8,128)(2,1)S(1)}, bf16[416,256]{1,0:T(8,128)(2,1)S(1)}, u32[]{:S(2)}, u32[]{:S(2)}) collective-permute-start(bf16[416,256]{1,0:T(8,128)(2,1)S(1)} %packed.1.block), channel_id=1, source_target_pairs={{0,8},{4,124},{8,16},{12,4},{16,24},{20,12},{24,32},{28,20},{32,40... | collective-permute-start | bytes 638984 | tf_op jit(solution)/shard_map/ppermute | solution.py:258
  28.1 3.1 %collective-permute-start.3 = (bf16[416,256]{1,0:T(8,128)(2,1)S(1)}, bf16[416,256]{1,0:T(8,128)(2,1)S(1)}, u32[]{:S(2)}, u32[]{:S(2)}) collective-permute-start(bf16[416,256]{1,0:T(8,128)(2,1)S(1)} %collective-permute-done.2.refs_0_), channel_id=1, source_target_pairs={{0,8},{4,124},{8,16},{12,4},{16,24},{20,12},{24,32},{28,20},{32,40... | collective-permute-start | bytes 638984 | tf_op jit(solution)/shard_map/ppermute | solution.py:258
  31.2 2.3 collective-permute-start.12
  34.0 3.1 %collective-permute-start.4 = (bf16[416,256]{1,0:T(8,128)(2,1)S(1)}, bf16[416,256]{1,0:T(8,128)(2,1)S(1)}, u32[]{:S(2)}, u32[]{:S(2)}) collective-permute-start(bf16[416,256]{1,0:T(8,128)(2,1)S(1)} %collective-permute-done.3.refs_0_), channel_id=1, source_target_pairs={{0,8},{4,124},{8,16},{12,4},{16,24},{20,12},{24,32},{28,20},{32,40... | collective-permute-start | bytes 638984 | tf_op jit(solution)/shard_map/ppermute | solution.py:258
  37.1 2.3 collective-permute-start.13
  39.9 3.1 %collective-permute-start.5 = (bf16[416,256]{1,0:T(8,128)(2,1)S(1)}, bf16[416,256]{1,0:T(8,128)(2,1)S(1)}, u32[]{:S(2)}, u32[]{:S(2)}) collective-permute-start(bf16[416,256]{1,0:T(8,128)(2,1)S(1)} %collective-permute-done.4.refs_2_), channel_id=1, source_target_pairs={{0,8},{4,124},{8,16},{12,4},{16,24},{20,12},{24,32},{28,20},{32,40... | collective-permute-start | bytes 638984 | tf_op jit(solution)/shard_map/ppermute | solution.py:258
  43.0 2.3 collective-permute-start.14
  45.8 3.1 %collective-permute-start.6 = (bf16[416,256]{1,0:T(8,128)(2,1)S(1)}, bf16[416,256]{1,0:T(8,128)(2,1)S(1)}, u32[]{:S(2)}, u32[]{:S(2)}) collective-permute-start(bf16[416,256]{1,0:T(8,128)(2,1)S(1)} %collective-permute-done.5.refs_0_), channel_id=1, source_target_pairs={{0,8},{4,124},{8,16},{12,4},{16,24},{20,12},{24,32},{28,20},{32,40... | collective-permute-start | bytes 638984 | tf_op jit(solution)/shard_map/ppermute | solution.py:258
  48.9 2.3 collective-permute-start.15
  51.7 3.1 %collective-permute-start.7 = (bf16[416,256]{1,0:T(8,128)(2,1)S(1)}, bf16[416,256]{1,0:T(8,128)(2,1)S(1)}, u32[]{:S(2)}, u32[]{:S(2)}) collective-permute-start(bf16[416,256]{1,0:T(8,128)(2,1)S(1)} %collective-permute-done.6.refs_2_), channel_id=1, source_target_pairs={{0,8},{4,124},{8,16},{12,4},{16,24},{20,12},{24,32},{28,20},{32,40... | collective-permute-start | bytes 638984 | tf_op jit(solution)/shard_map/ppermute | solution.py:258
  54.8 2.3 collective-permute-start.16
  57.6 3.1 %collective-permute-start.8 = (bf16[416,256]{1,0:T(8,128)(2,1)S(1)}, bf16[416,256]{1,0:T(8,128)(2,1)S(1)}, u32[]{:S(2)}, u32[]{:S(2)}) collective-permute-start(bf16[416,256]{1,0:T(8,128)(2,1)S(1)} %collective-permute-done.7.refs_0_), channel_id=1, source_target_pairs={{0,8},{4,124},{8,16},{12,4},{16,24},{20,12},{24,32},{28,20},{32,40... | collective-permute-start | bytes 638984 | tf_op jit(solution)/shard_map/ppermute | solution.py:258
  60.7 4.1 %collective-permute-start = (bf16[256,256]{1,0:T(8,128)(2,1)}, bf16[256,256]{1,0:T(8,128)(2,1)S(1)}, u32[]{:S(2)}, u32[]{:S(2)}) collective-permute-start(bf16[256,256]{1,0:T(8,128)(2,1)} %own_s.1), channel_id=1, source_target_pairs={{0,4},{4,0},{8,12},{12,8},{16,20},{20,16},{24,28},{28,24},{32,36},... | collective-permute-start | bytes 393224 | tf_op jit(solution)/shard_map/ppermute | solution.py:247
  64.8 3.0 %collective-permute-start.17 = (bf16[416,256]{1,0:T(8,128)(2,1)S(1)}, bf16[416,256]{1,0:T(8,128)(2,1)S(1)}, u32[]{:S(2)}, u32[]{:S(2)}) collective-permute-start(bf16[416,256]{1,0:T(8,128)(2,1)S(1)} %collective-permute-done.16.refs_1_), channel_id=1, source_target_pairs={{0,8},{4,124},{8,16},{12,4},{16,24},{20,12},{24,32},{28,20},{32,40... | collective-permute-start | bytes 638984 | tf_op jit(solution)/shard_map/ppermute | solution.py:262
  69.8 3.7 %first.1 = (bf16[4,80,256]{2,1,0:T(8,128)(2,1)S(1)}, bf16[2,144,256]{2,1,0:T(8,128)(2,1)S(1)}, bf16[4,80,256]{2,1,0:T(8,128)(2,1)S(1)}, bf16[2,144,256]{2,1,0:T(...) custom-call(s32[9]{0:T(128)S(1)} %pad_add_fusion.info.flags, ...), custom_call_target="tpu_custom_call" | custom-call | tf_op jit(solution)/shard_map/first/pallas_call | solution.py:170
  76.4 6.4 %collective-permute-start.18 = (f32[4,88,256]{2,1,0:T(8,128)S(1)}, f32[4,88,256]{2,1,0:T(8,128)S(1)}, u32[]{:S(2)}, u32[]{:S(2)}) collective-permute-start(f32[4,88,256]{2,1,0:T(8,128)S(1)} %get-tuple-element.61), channel_id=1, source_target_pairs={{0,4},{4,0},{8,12},{12,8},{16,20},{20,16},{24,28},{28,24},{32,36},... | collective-permute-start | bytes 1081352 | tf_op jit(solution)/shard_map/ppermute | solution.py:268
  86.4 4.4 %all-to-all-start = ((bf16[4,64,2048]{2,1,0:T(8,128)(2,1)}), bf16[4,64,2048]{2,1,0:T(8,128)(2,1)S(1)}, u32[]{:S(2)}, u32[]{:S(2)}) async-start(bf16[4,64,2048]{2,1,0:T(8,128)(2,1)} %bitcast.1), calls=%async_computation | async-start | bytes 2097152 | tf_op jit(solution)/shard_map/all_to_all | solution.py:437
  91.7 13.6 %all-to-all-done.parts = bf16[4,64,2048]{2,1,0:T(8,128)(2,1)S(1)} async-done(((bf16[4,64,2048]{2,1,0:T(8,128)(2,1)}), bf16[4,64,2048]{2,1,0:T(8,128)(2,1)S(1)}, u32[]{:S(2)}, u32[]{:S(2)}) %all-to-all-start) | async-done | bytes 1048608 | tf_op jit(solution)/shard_map/all_to_all | solution.py:437
  106.8 91.4 %all_to_all.15 = bf16[128,2,2048]{2,1,0:T(2,128)(2,1)S(1)} all-to-all(bf16[128,2,2048]{2,1,0:T(2,128)(2,1)S(1)} %reshape.70), channel_id=1, replica_groups=mesh['grp'=2,'sp'=32,'tp'=4] {'sp','tp'}, dimensions={0} | all-to-all | bytes 2097152 | tf_op jit(solution)/shard_map/all_to_all | solution.py:440
  199.4 7.1 %expert.1 = bf16[256,2048]{1,0:T(8,128)(2,1)} custom-call(bf16[256,2048]{1,0:T(8,128)(2,1)} %reshape.71.rows, bf16[1,2048,512]{2,1,0:T(8,128)(2,1)} %gate.1, bf16[1,2048,512]{2,1,0:T(8,128)(2,1)} %up.1, bf16[1,512,2048]{2,1,0:T(8,128)(2,1)} %down.1), custom_call_target="tpu_custom_call" | custom-call | tf_op jit(solution)/shard_map/expert/pallas_call | solution.py:344
  206.5 2.5 reshape.72
  209.0 8.5 %all-to-all-start.2 = ((bf16[128,2,2048]{2,1,0:T(2,128)(2,1)}), bf16[128,2,2048]{2,1,0:T(2,128)(2,1)}, u32[]{:S(2)}, u32[]{:S(2)}) async-start(bf16[128,2,2048]{2,1,0:T(2,128)(2,1)} %reshape.72), calls=%async_computation.2 | async-start | bytes 2097152 | tf_op jit(solution)/shard_map/all_to_all | solution.py:443
  217.7 54.2 %all-to-all-done.2 = bf16[128,2,2048]{2,1,0:T(2,128)(2,1)} async-done(((bf16[128,2,2048]{2,1,0:T(2,128)(2,1)}), bf16[128,2,2048]{2,1,0:T(2,128)(2,1)}, u32[]{:S(2)}, u32[]{:S(2)}) %all-to-all-start.2) | async-done | bytes 1048608 | tf_op jit(solution)/shard_map/all_to_all | solution.py:443
  (69 shorter events, 21.8 us)
Async XLA Ops:
  1.6 23.6 %collective-permute-start.10 = (bf16[416,256]{1,0:T(8,128)(2,1)S(1)}, bf16[416,256]{1,0:T(8,128)(2,1)S(1)}, u32[]{:S(2)}, u32[]{:S(2)}) collective-permute-start(bf16[416,256]{1,0:T(8,128)(2,1)S(1)} %packed.1.block), channel_id=1, source_target_pairs={{0,4},{4,0},{8,12},{12,8},{16,20},{20,16},{24,28},{28,24},{32,36},... | collective-permute-start | bytes 638984 | tf_op jit(solution)/shard_map/ppermute | solution.py:252
  22.2 5.9 %collective-permute-start.2 = (bf16[416,256]{1,0:T(8,128)(2,1)S(1)}, bf16[416,256]{1,0:T(8,128)(2,1)S(1)}, u32[]{:S(2)}, u32[]{:S(2)}) collective-permute-start(bf16[416,256]{1,0:T(8,128)(2,1)S(1)} %packed.1.block), channel_id=1, source_target_pairs={{0,8},{4,124},{8,16},{12,4},{16,24},{20,12},{24,32},{28,20},{32,40... | collective-permute-start | bytes 638984 | tf_op jit(solution)/shard_map/ppermute | solution.py:258
  25.3 5.9 %collective-permute-start.11 = (bf16[416,256]{1,0:T(8,128)(2,1)S(1)}, bf16[416,256]{1,0:T(8,128)(2,1)S(1)}, u32[]{:S(2)}, u32[]{:S(2)}) collective-permute-start(bf16[416,256]{1,0:T(8,128)(2,1)S(1)} %collective-permute-done.10), channel_id=1, source_target_pairs={{0,8},{4,124},{8,16},{12,4},{16,24},{20,12},{24,32},{28,20},{32,40... | collective-permute-start | bytes 638984 | tf_op jit(solution)/shard_map/ppermute | solution.py:262
  28.1 5.9 %collective-permute-start.3 = (bf16[416,256]{1,0:T(8,128)(2,1)S(1)}, bf16[416,256]{1,0:T(8,128)(2,1)S(1)}, u32[]{:S(2)}, u32[]{:S(2)}) collective-permute-start(bf16[416,256]{1,0:T(8,128)(2,1)S(1)} %collective-permute-done.2.refs_0_), channel_id=1, source_target_pairs={{0,8},{4,124},{8,16},{12,4},{16,24},{20,12},{24,32},{28,20},{32,40... | collective-permute-start | bytes 638984 | tf_op jit(solution)/shard_map/ppermute | solution.py:258
  31.2 5.9 %collective-permute-start.12 = (bf16[416,256]{1,0:T(8,128)(2,1)S(1)}, bf16[416,256]{1,0:T(8,128)(2,1)S(1)}, u32[]{:S(2)}, u32[]{:S(2)}) collective-permute-start(bf16[416,256]{1,0:T(8,128)(2,1)S(1)} %collective-permute-done.11.refs_1_), channel_id=1, source_target_pairs={{0,8},{4,124},{8,16},{12,4},{16,24},{20,12},{24,32},{28,20},{32,40... | collective-permute-start | bytes 638984 | tf_op jit(solution)/shard_map/ppermute | solution.py:262
  34.0 5.9 %collective-permute-start.4 = (bf16[416,256]{1,0:T(8,128)(2,1)S(1)}, bf16[416,256]{1,0:T(8,128)(2,1)S(1)}, u32[]{:S(2)}, u32[]{:S(2)}) collective-permute-start(bf16[416,256]{1,0:T(8,128)(2,1)S(1)} %collective-permute-done.3.refs_0_), channel_id=1, source_target_pairs={{0,8},{4,124},{8,16},{12,4},{16,24},{20,12},{24,32},{28,20},{32,40... | collective-permute-start | bytes 638984 | tf_op jit(solution)/shard_map/ppermute | solution.py:258
  37.1 5.9 %collective-permute-start.13 = (bf16[416,256]{1,0:T(8,128)(2,1)S(1)}, bf16[416,256]{1,0:T(8,128)(2,1)S(1)}, u32[]{:S(2)}, u32[]{:S(2)}) collective-permute-start(bf16[416,256]{1,0:T(8,128)(2,1)S(1)} %collective-permute-done.12.refs_1_), channel_id=1, source_target_pairs={{0,8},{4,124},{8,16},{12,4},{16,24},{20,12},{24,32},{28,20},{32,40... | collective-permute-start | bytes 638984 | tf_op jit(solution)/shard_map/ppermute | solution.py:262
  39.9 5.9 %collective-permute-start.5 = (bf16[416,256]{1,0:T(8,128)(2,1)S(1)}, bf16[416,256]{1,0:T(8,128)(2,1)S(1)}, u32[]{:S(2)}, u32[]{:S(2)}) collective-permute-start(bf16[416,256]{1,0:T(8,128)(2,1)S(1)} %collective-permute-done.4.refs_2_), channel_id=1, source_target_pairs={{0,8},{4,124},{8,16},{12,4},{16,24},{20,12},{24,32},{28,20},{32,40... | collective-permute-start | bytes 638984 | tf_op jit(solution)/shard_map/ppermute | solution.py:258
  43.0 5.9 %collective-permute-start.14 = (bf16[416,256]{1,0:T(8,128)(2,1)S(1)}, bf16[416,256]{1,0:T(8,128)(2,1)S(1)}, u32[]{:S(2)}, u32[]{:S(2)}) collective-permute-start(bf16[416,256]{1,0:T(8,128)(2,1)S(1)} %collective-permute-done.13.refs_3_), channel_id=1, source_target_pairs={{0,8},{4,124},{8,16},{12,4},{16,24},{20,12},{24,32},{28,20},{32,40... | collective-permute-start | bytes 638984 | tf_op jit(solution)/shard_map/ppermute | solution.py:262
  45.8 5.9 %collective-permute-start.6 = (bf16[416,256]{1,0:T(8,128)(2,1)S(1)}, bf16[416,256]{1,0:T(8,128)(2,1)S(1)}, u32[]{:S(2)}, u32[]{:S(2)}) collective-permute-start(bf16[416,256]{1,0:T(8,128)(2,1)S(1)} %collective-permute-done.5.refs_0_), channel_id=1, source_target_pairs={{0,8},{4,124},{8,16},{12,4},{16,24},{20,12},{24,32},{28,20},{32,40... | collective-permute-start | bytes 638984 | tf_op jit(solution)/shard_map/ppermute | solution.py:258
  48.9 5.9 %collective-permute-start.15 = (bf16[416,256]{1,0:T(8,128)(2,1)S(1)}, bf16[416,256]{1,0:T(8,128)(2,1)S(1)}, u32[]{:S(2)}, u32[]{:S(2)}) collective-permute-start(bf16[416,256]{1,0:T(8,128)(2,1)S(1)} %collective-permute-done.14.refs_1_), channel_id=1, source_target_pairs={{0,8},{4,124},{8,16},{12,4},{16,24},{20,12},{24,32},{28,20},{32,40... | collective-permute-start | bytes 638984 | tf_op jit(solution)/shard_map/ppermute | solution.py:262
  51.7 5.9 %collective-permute-start.7 = (bf16[416,256]{1,0:T(8,128)(2,1)S(1)}, bf16[416,256]{1,0:T(8,128)(2,1)S(1)}, u32[]{:S(2)}, u32[]{:S(2)}) collective-permute-start(bf16[416,256]{1,0:T(8,128)(2,1)S(1)} %collective-permute-done.6.refs_2_), channel_id=1, source_target_pairs={{0,8},{4,124},{8,16},{12,4},{16,24},{20,12},{24,32},{28,20},{32,40... | collective-permute-start | bytes 638984 | tf_op jit(solution)/shard_map/ppermute | solution.py:258
  54.8 10.0 %collective-permute-start.16 = (bf16[416,256]{1,0:T(8,128)(2,1)S(1)}, bf16[416,256]{1,0:T(8,128)(2,1)S(1)}, u32[]{:S(2)}, u32[]{:S(2)}) collective-permute-start(bf16[416,256]{1,0:T(8,128)(2,1)S(1)} %collective-permute-done.15.refs_3_), channel_id=1, source_target_pairs={{0,8},{4,124},{8,16},{12,4},{16,24},{20,12},{24,32},{28,20},{32,40... | collective-permute-start | bytes 638984 | tf_op jit(solution)/shard_map/ppermute | solution.py:262
  57.6 10.2 %collective-permute-start.8 = (bf16[416,256]{1,0:T(8,128)(2,1)S(1)}, bf16[416,256]{1,0:T(8,128)(2,1)S(1)}, u32[]{:S(2)}, u32[]{:S(2)}) collective-permute-start(bf16[416,256]{1,0:T(8,128)(2,1)S(1)} %collective-permute-done.7.refs_0_), channel_id=1, source_target_pairs={{0,8},{4,124},{8,16},{12,4},{16,24},{20,12},{24,32},{28,20},{32,40... | collective-permute-start | bytes 638984 | tf_op jit(solution)/shard_map/ppermute | solution.py:258
  60.7 7.3 %collective-permute-start = (bf16[256,256]{1,0:T(8,128)(2,1)}, bf16[256,256]{1,0:T(8,128)(2,1)S(1)}, u32[]{:S(2)}, u32[]{:S(2)}) collective-permute-start(bf16[256,256]{1,0:T(8,128)(2,1)} %own_s.1), channel_id=1, source_target_pairs={{0,4},{4,0},{8,12},{12,8},{16,20},{20,16},{24,28},{28,24},{32,36},... | collective-permute-start | bytes 393224 | tf_op jit(solution)/shard_map/ppermute | solution.py:247
  64.8 3.2 %collective-permute-start.1 = (bf16[256,256]{1,0:T(8,128)(2,1)}, bf16[256,256]{1,0:T(8,128)(2,1)}, u32[]{:S(2)}, u32[]{:S(2)}) collective-permute-start(bf16[256,256]{1,0:T(8,128)(2,1)} %own_l.1), channel_id=1, source_target_pairs={{0,4},{4,0},{8,12},{12,8},{16,20},{20,16},{24,28},{28,24},{32,36},... | collective-permute-start | bytes 393224 | tf_op jit(solution)/shard_map/ppermute | solution.py:248
  64.8 10.4 %collective-permute-start.17 = (bf16[416,256]{1,0:T(8,128)(2,1)S(1)}, bf16[416,256]{1,0:T(8,128)(2,1)S(1)}, u32[]{:S(2)}, u32[]{:S(2)}) collective-permute-start(bf16[416,256]{1,0:T(8,128)(2,1)S(1)} %collective-permute-done.16.refs_1_), channel_id=1, source_target_pairs={{0,8},{4,124},{8,16},{12,4},{16,24},{20,12},{24,32},{28,20},{32,40... | collective-permute-start | bytes 638984 | tf_op jit(solution)/shard_map/ppermute | solution.py:262
  67.8 8.0 %collective-permute-start.9 = (bf16[416,256]{1,0:T(8,128)(2,1)S(1)}, bf16[416,256]{1,0:T(8,128)(2,1)S(1)}, u32[]{:S(2)}, u32[]{:S(2)}) collective-permute-start(bf16[416,256]{1,0:T(8,128)(2,1)S(1)} %collective-permute-done.8.refs_2_), channel_id=1, source_target_pairs={{0,8},{4,124},{8,16},{12,4},{16,24},{20,12},{24,32},{28,20},{32,40... | collective-permute-start | bytes 638984 | tf_op jit(solution)/shard_map/ppermute | solution.py:258
  76.4 8.2 %collective-permute-start.18 = (f32[4,88,256]{2,1,0:T(8,128)S(1)}, f32[4,88,256]{2,1,0:T(8,128)S(1)}, u32[]{:S(2)}, u32[]{:S(2)}) collective-permute-start(f32[4,88,256]{2,1,0:T(8,128)S(1)} %get-tuple-element.61), channel_id=1, source_target_pairs={{0,4},{4,0},{8,12},{12,8},{16,20},{20,16},{24,28},{28,24},{32,36},... | collective-permute-start | bytes 1081352 | tf_op jit(solution)/shard_map/ppermute | solution.py:268
  82.9 1.7 collective-permute-start.19
  86.4 19.0 %copy-start.2 = (bf16[64,2048]{1,0:T(8,128)(2,1)S(1)}, bf16[64,2048]{1,0:T(8,128)(2,1)}, u32[]{:S(2)}) copy-start(bf16[64,2048]{1,0:T(8,128)(2,1)} %residual_in.1) | copy-start | bytes 786436
  86.4 19.0 %all-to-all-start = ((bf16[4,64,2048]{2,1,0:T(8,128)(2,1)}), bf16[4,64,2048]{2,1,0:T(8,128)(2,1)S(1)}, u32[]{:S(2)}, u32[]{:S(2)}) async-start(bf16[4,64,2048]{2,1,0:T(8,128)(2,1)} %bitcast.1), calls=%async_computation | async-start | bytes 2097152 | tf_op jit(solution)/shard_map/all_to_all | solution.py:437
  206.5 11.1 %copy-start.7 = (f32[64,2]{0,1:T(2,128)S(1)}, f32[64,2]{0,1:T(2,128)}, u32[]{:S(2)}) copy-start(f32[64,2]{0,1:T(2,128)} %param.33) | copy-start | bytes 1540
  209.0 62.9 %all-to-all-start.2 = ((bf16[128,2,2048]{2,1,0:T(2,128)(2,1)}), bf16[128,2,2048]{2,1,0:T(2,128)(2,1)}, u32[]{:S(2)}, u32[]{:S(2)}) async-start(bf16[128,2,2048]{2,1,0:T(2,128)(2,1)} %reshape.72), calls=%async_computation.2 | async-start | bytes 2097152 | tf_op jit(solution)/shard_map/all_to_all | solution.py:443
  (6 other events, 30.3 us)
